TPU v7x, 512 devices: a whole 4x8x8 slice. The times are simulated.
512 devices in a mesh: sp: 64 (over z, y), fs: 4 (over x), tp: 2 (over core).
Axes of the slice: x: 4, y: 8, z: 8, core: 2. Of those that a mesh axis runs over, the one named last changes fastest.
Arguments:
- tokens: bfloat16 [32768, 2048], P(('fs', 'sp')), parts along dimension 0, may hold values from -6 to 6
- norm_gain: bfloat16 [2048], replicated, may hold values from 0.099609375 to 1.8984375
- query_down: bfloat16 [2048, 512], P('sp'), may hold values from -0.125 to 0.125
- query_gain: bfloat16 [512], replicated, may hold values from 0.099609375 to 1.8984375
- latent_down: bfloat16 [2048, 256], replicated, may hold values from -0.125 to 0.125
- latent_gain: bfloat16 [256], replicated, may hold values from 0.099609375 to 1.8984375
- rope_down: bfloat16 [2048, 64], replicated, may hold values from -30 to 30
- query_up: bfloat16 [512, 1536], P(None, 'tp'), may hold values from -0.25 to 0.25
- key_up: bfloat16 [256, 1024], P(None, 'tp'), may hold values from -0.75 to 0.75
- value_up: bfloat16 [256, 1024], P(None, 'tp'), may hold values from -0.375 to 0.375
- glu_value: bfloat16 [2048, 1024], P('sp', 'tp'), may hold values from -0.125 to 0.125
- glu_gate: bfloat16 [2048, 1024], P('sp', 'tp'), may hold values from -0.125 to 0.125
- conv_taps: bfloat16 [31, 1024], P(None, 'tp'), may hold values from -1 to 1
- group_gain: bfloat16 [1024], P('tp'), may hold values from 0.099609375 to 1.8984375
- head_proj: bfloat16 [1024, 2048], P('tp', 'sp'), may hold values from -0.75 to 0.75
- channel_proj: bfloat16 [1024, 2048], P('tp', 'sp'), may hold values from -0.1875 to 0.1875
Outputs:
- mixed_out: bfloat16 [32768, 2048], P(('fs', 'sp'), 'tp'), parts along dimension 0
- log_weight: float32 [8, 32768], P('tp', ('fs', 'sp')), parts along dimension 1
There are 4 independent parts, one for each index of `fs`. A program takes and returns all parts, laid end to end along the dimension named above; an argument that names none is the same for every part. Nothing has to cross between parts.
All inputs are finite; a program needn't handle non-finite values.
Results may differ from a plain program's by a relative error of at most 0.015.
The roundings to bfloat16 on the way count: a program that leaves them out, or rounds other values in their place, can miss the bound.
Values may be sent and summed in bfloat16 or wider, within the bound.
No kernel may reach another device: no remote copies, remote signals or barrier semaphores. Data moves between devices by JAX's collectives and lax.ppermute only.
A program may use at most 128 MiB of HBM per device.

v0:
```python
import jax
import jax.numpy as jnp
from jax import lax
from jax.sharding import PartitionSpec as P

NOPE = 128
ROPE = 64
VDIM = 128
KVR = 256
CH = 1024
GROUPS = 8
GRID_W = 64
norm_eps = 1e-06
rope_base = 10000.0
far_below = -1e30


def in_one_piece(arrays, axis, dim, along):
    widths = [a.shape[along] for a in arrays]
    both = jnp.concatenate(arrays, axis=along)
    result = lax.all_gather(both, axis, axis=dim, tiled=True)
    return tuple(jnp.split(result, [sum(widths[:k]) for k in range(1, len(widths))], axis=along))


def padded_2(block, sides, width):
    for axis, dim in sides:
        count = lax.axis_size(axis)
        forward = [(i, i + 1) for i in range(count - 1)]
        backward = [(target, source) for source, target in forward]
        low = lax.ppermute(
            lax.slice_in_dim(block, block.shape[dim] - width, None, axis=dim), axis, forward
        )
        high = lax.ppermute(lax.slice_in_dim(block, 0, width, axis=dim), axis, backward)
        block = jnp.concatenate([low, block, high], axis=dim)
    return block


def split_up(shard, dim, length):
    before, after = (shard.shape[:dim], shard.shape[dim + 1 :])
    return jnp.moveaxis(shard.reshape(*before, length, -1, *after), dim, 0)


def sent_and_summed(shard, axis, dim):
    tiles = split_up(shard, dim, lax.axis_size(axis))
    arrived = lax.all_to_all(tiles, axis, split_axis=0, concat_axis=0, tiled=True)
    return arrived.astype(jnp.float32).sum(axis=0)


def rms_scale(values, scale_gain):
    inv_rms = lax.rsqrt(jnp.mean(values * values, axis=-1, keepdims=True) + norm_eps)
    return values * inv_rms * scale_gain.astype(jnp.float32)


def angles_for(positions, rope_size):
    quarter = rope_size // 4
    inverse = rope_base ** (-jnp.arange(quarter, dtype=jnp.float32) / quarter)
    grid_row = (positions // GRID_W).astype(jnp.float32)
    grid_col = (positions % GRID_W).astype(jnp.float32)
    return jnp.concatenate([grid_row[:, None] * inverse, grid_col[:, None] * inverse], axis=-1)


def rotate(values, angles):
    half_size = values.shape[-1] // 2
    front_half = values[..., :half_size]
    back_half = values[..., half_size:]
    cosine = jnp.cos(angles)
    sine_part = jnp.sin(angles)
    return jnp.concatenate(
        [front_half * cosine - back_half * sine_part, back_half * cosine + front_half * sine_part],
        axis=-1,
    )


def key_block(normed, latent_down, latent_gain, rope_down, positions):
    latent = jnp.dot(normed, latent_down, preferred_element_type=jnp.float32)
    latent = rms_scale(latent, latent_gain).astype(jnp.bfloat16)
    rope_key = jnp.dot(normed, rope_down, preferred_element_type=jnp.float32)
    rope_key = rotate(rope_key, angles_for(positions, rope_key.shape[-1])).astype(jnp.bfloat16)
    return jnp.concatenate([latent, rope_key], axis=1)


def per_device(
    tokens,
    norm_gain,
    query_down,
    query_gain,
    latent_down,
    latent_gain,
    rope_down,
    query_up,
    key_up,
    value_up,
    glu_value,
    glu_gate,
    conv_taps,
    group_gain,
    head_proj,
    channel_proj,
):
    tok_count = tokens.shape[0]
    reach_rows = conv_taps.shape[0] // 2
    head_count = key_up.shape[1] // NOPE
    normed = rms_scale(tokens.astype(jnp.float32), norm_gain).astype(jnp.bfloat16)
    offsets = lax.axis_index("sp") * tok_count + jnp.arange(tok_count, dtype=jnp.int32)
    blocks = in_one_piece((query_down, glu_value, glu_gate), "sp", 0, 1)
    query_latent = jnp.dot(normed, blocks[0], preferred_element_type=jnp.float32)
    value_in = jnp.dot(normed, blocks[1], preferred_element_type=jnp.float32)
    gate_in = jnp.dot(normed, blocks[2], preferred_element_type=jnp.float32)
    latent_query = rms_scale(query_latent, query_gain).astype(jnp.bfloat16)
    query_all = jnp.dot(latent_query, query_up, preferred_element_type=jnp.float32).reshape(
        tok_count, head_count, NOPE + ROPE
    )
    query_plain = query_all[:, :, :NOPE].astype(jnp.bfloat16)
    query_rope = rotate(query_all[:, :, NOPE:], angles_for(offsets, ROPE)[:, None, :]).astype(
        jnp.bfloat16
    )
    absorbed = jnp.einsum(
        "thd,rhd->htr",
        query_plain,
        key_up.reshape(KVR, head_count, NOPE),
        preferred_element_type=jnp.float32,
    ).astype(jnp.bfloat16)
    queries = jnp.concatenate([absorbed, jnp.transpose(query_rope, (1, 0, 2))], axis=-1)
    score_scale = (NOPE + ROPE) ** (-0.5)
    half_rows = tok_count // lax.axis_size("tp")
    first_row = lax.axis_index("tp") * half_rows
    own_rows = lax.dynamic_slice_in_dim(normed, first_row, half_rows, 0)
    own_positions = lax.dynamic_slice_in_dim(offsets, first_row, half_rows, 0)
    own_keys = key_block(own_rows, latent_down, latent_gain, rope_down, own_positions)
    block_keys = lax.all_gather(own_keys, ("sp", "tp"), axis=0, tiled=True)
    row_max = jnp.full((head_count, tok_count), far_below, jnp.float32)
    scores = (
        jnp.einsum("hqc,kc->hqk", queries, block_keys, preferred_element_type=jnp.float32)
        * score_scale
    )
    new_max = jnp.maximum(row_max, jnp.max(scores, axis=2))
    weights = jnp.exp(scores - new_max[:, :, None])
    new_sum = jnp.sum(weights, axis=2)
    added = jnp.einsum(
        "hqk,kr->hqr",
        weights.astype(jnp.bfloat16),
        block_keys[:, :KVR],
        preferred_element_type=jnp.float32,
    )
    gated_rows = (value_in * jax.nn.sigmoid(gate_in)).astype(jnp.bfloat16)
    padded = padded_2(gated_rows, (("sp", 0),), reach_rows)
    filtered = padded[0:tok_count].astype(jnp.float32) * conv_taps[0].astype(jnp.float32)
    for tap_index in range(1, conv_taps.shape[0]):
        filtered = filtered + padded[tap_index : tap_index + tok_count].astype(
            jnp.float32
        ) * conv_taps[tap_index].astype(jnp.float32)
    grouped = filtered.reshape(tok_count, -1, CH // GROUPS)
    centred = grouped - jnp.mean(grouped, axis=-1, keepdims=True)
    spread = jnp.mean(centred * centred, axis=-1, keepdims=True)
    normal_groups = (centred * lax.rsqrt(spread + norm_eps)).reshape(tok_count, -1)
    conv_branch = jax.nn.silu(normal_groups * group_gain.astype(jnp.float32)).astype(jnp.bfloat16)
    attended = (added / new_sum[:, :, None]).astype(jnp.bfloat16)
    log_weight = new_max + jnp.log(new_sum)
    head_out = jnp.einsum(
        "htr,rhv->thv",
        attended,
        value_up.reshape(KVR, head_count, VDIM),
        preferred_element_type=jnp.float32,
    )
    head_out = head_out.reshape(tok_count, head_count * VDIM).astype(jnp.bfloat16)
    mixed_in = jnp.concatenate([head_out, conv_branch], axis=1)
    out_weight = jnp.concatenate([head_proj, channel_proj], axis=0)
    partial_terms = jnp.dot(
        mixed_in,
        lax.all_gather(out_weight, "sp", axis=1, tiled=True),
        preferred_element_type=jnp.float32,
    )
    mixed_out = sent_and_summed(partial_terms.astype(jnp.bfloat16), "tp", 1).astype(jnp.bfloat16)
    return (mixed_out, log_weight)


def solution(mesh):
    in_specs = (
        P(("fs", "sp"), None),
        P(),
        P("sp", None),
        P(),
        P(),
        P(),
        P(),
        P(None, "tp"),
        P(None, "tp"),
        P(None, "tp"),
        P("sp", "tp"),
        P("sp", "tp"),
        P(None, "tp"),
        P("tp"),
        P("tp", "sp"),
        P("tp", "sp"),
    )
    out_specs = (P(("fs", "sp"), "tp"), P("tp", ("fs", "sp")))
    return jax.shard_map(
        per_device, mesh=mesh, in_specs=in_specs, out_specs=out_specs, check_vma=False
    )
```

profile of v0, /device:TPU:1, one launch (start us, length us, event | category | flops | bytes accessed | tf_op | source)
XLA Modules:
  0.0 295.6 jit_solution(11499413010207656620)
XLA Ops:
  7.2 1.5 pad_maximum_fusion.2
  10.3 1.2 fusion.32
  11.5 1.2 fusion.34
  13.3 1.2 fusion.53
  14.7 0.7 pad_maximum_fusion.4
  15.5 1.4 pad_maximum_fusion.3
  18.7 1.1 copy.70
  19.8 1.0 slice_convert_fusion.31
  20.8 1.0 slice_convert_fusion.32
  21.8 84.6 %all-gather.4.cloned.1.call-done = bf16[2048,1536]{1,0:T(8,128)(2,1)} async-done(((bf16[32,1536]{1,0:T(8,128)(2,1)}), bf16[2048,1536]{1,0:T(8,128)(2,1)}) %all-gather.4.cloned.1.call-update) | async-done | bytes 6291472 | tf_op jit(solution)/shard_map/all_gather | solution.py:21
  106.4 2.1 fusion.26
  108.5 2.1 fusion.29
  110.6 1.9 collective-permute-start
  112.6 1.3 collective-permute-start.1
  113.9 2.1 multiply_reduce_fusion.2
  117.3 76.4 %all-gather.6.cloned.1.call-done = bf16[8192,320]{1,0:T(8,128)(2,1)} async-done(((bf16[64,320]{1,0:T(8,128)(2,1)}), bf16[8192,320]{1,0:T(8,128)(2,1)}) %all-gather.6.cloned.1.call-update) | async-done | bytes 5242896 | tf_op jit(solution)/shard_map/all_gather | solution.py:130
  193.6 10.9 %multiply_reduce_fusion = (f32[4,128]{1,0:T(4,128)S(1)}, f32[4,128,8192]{2,1,0:T(8,128)}) fusion(bf16[8192,320]{1,0:T(8,128)(2,1)} %all-gather.6.cloned.1.call-done, bf16[4,128,64]{2,1,0:T(8,128)(2,1)S(1)} %maximum_bitcast_fusion, bf16[4,128,256]{2,1,0:T(8,128)(2,1)S(1)} %convolution_convert_fusion.1), kind=kOutput, calls=%fused_computation.1 | convolution fusion | flops 2693398016 | bytes 22349824 | tf_op jit(solution)/shard_map/hqc,kc->hqk/dot_general | solution.py:133
  204.5 8.7 %fusion = f32[4,128]{1,0:T(4,128)S(1)} fusion(f32[4,128,8192]{2,1,0:T(8,128)} %get-tuple-element.54, f32[4,128]{1,0:T(4,128)S(1)} %broadcast_maximum_fusion), kind=kLoop, calls=%fused_computation.2 | loop fusion | flops 12582400 | bytes 16781312 | tf_op jit(solution)/shard_map/reduce_sum | solution.py:138
  213.2 9.9 %convolution_convert_fusion.2 = bf16[4,128,128]{1,2,0:T(8,128)(2,1)S(1)} fusion(bf16[256,4,128]{0,2,1:T(8,128)(2,1)S(1)} %bitcast.94, bf16[8192,320]{1,0:T(8,128)(2,1)} %all-gather.6.cloned.1.call-done, f32[4,128,8192]{2,1,0:T(8,128)} %get-tuple-element.54, f32[4,128]{1,0:T(4,128)S(1)} %broadcast_maximum_fusion, f32[4,128]{1,0:T(4,128)S(1)} %fusion), kind=kOutput, calls=%fused_computation.26 | convolution fusion | flops 2193948672 | bytes 21368832 | tf_op jit(solution)/shard_map/htr,rhv->thv/dot_general | solution.py:159
  223.8 1.0 multiply_add_fusion
  226.0 49.8 %all-gather.8.cloned.1.call-done = bf16[1024,2048]{0,1:T(8,128)(2,1)} async-done(((bf16[1024,32]{0,1:T(8,128)(2,1)}), bf16[1024,2048]{0,1:T(8,128)(2,1)}) %all-gather.8.cloned.1.call-update) | async-done | bytes 4194320 | tf_op jit(solution)/shard_map/all_gather | solution.py:170
  275.9 3.7 %convolution_convert_fusion = bf16[128,2048]{1,0:T(8,128)(2,1)S(1)} fusion(bf16[1024,2048]{0,1:T(8,128)(2,1)} %all-gather.8.cloned.1.call-done, bf16[128,512]{1,0:T(8,128)(2,1)S(1)} %multiply_convert_fusion, bf16[128,512]{1,0:T(8,128)(2,1)S(1)} %copy.64), kind=kOutput, calls=%fused_computation.10 | convolution fusion | flops 537657344 | bytes 4980736 | tf_op jit(solution)/shard_map/dot_general | solution.py:168
  279.6 8.6 %all_to_all.5 = bf16[2,128,1024]{2,1,0:T(8,128)(2,1)S(1)} all-to-all(bf16[2,128,1024]{2,1,0:T(8,128)(2,1)S(1)} %bitcast.89), channel_id=1, replica_groups=mesh['sp'=64,'fs'=4,'tp'=2] {'tp'}, dimensions={0} | all-to-all | bytes 1048576 | tf_op jit(solution)/shard_map/all_to_all | solution.py:45
  288.2 0.8 reduce_sum.72
  (54 shorter events, 7.3 us)
Async XLA Ops:
  7.2 5.6 %copy-start = (bf16[2048,256]{1,0:T(8,128)(2,1)S(1)}, bf16[2048,256]{1,0:T(8,128)(2,1)}, u32[]{:S(2)}) copy-start(bf16[2048,256]{1,0:T(8,128)(2,1)} %param.20) | copy-start | bytes 3145732
  7.2 99.3 %all-gather.4.cloned.1.call-start = ((), (), s32[]{:S(2)}) async-start(), calls=%async_computation.1 | async-start | bytes 6389760 | tf_op jit(solution)/shard_map/all_gather | solution.py:21
  8.8 184.9 %all-gather.6.cloned.1.call-start = ((), (), s32[]{:S(2)}) async-start(), calls=%async_computation.2 | async-start | bytes 6340608 | tf_op jit(solution)/shard_map/all_gather | solution.py:130
  14.6 101.4 %copy-start.1 = (bf16[512,768]{1,0:T(8,128)(2,1)S(1)}, bf16[512,768]{1,0:T(8,128)(2,1)}, u32[]{:S(2)}) copy-start(bf16[512,768]{1,0:T(8,128)(2,1)} %param.23) | copy-start | bytes 2359300
  15.5 260.4 %all-gather.8.cloned.1.call-start = ((), (), s32[]{:S(2)}) async-start(), calls=%async_computation.3 | async-start | bytes 4259840 | tf_op jit(solution)/shard_map/all_gather | solution.py:170
  108.5 8.5 %copy-start.2 = (bf16[256,512]{1,0:T(8,128)(2,1)S(1)}, bf16[256,512]{1,0:T(8,128)(2,1)}, u32[]{:S(2)}) copy-start(bf16[256,512]{1,0:T(8,128)(2,1)} %param.24) | copy-start | bytes 786436
  110.6 113.2 %collective-permute-start = (bf16[15,512]{1,0:T(8,128)(2,1)S(1)}, bf16[15,512]{1,0:T(8,128)(2,1)S(1)}, u32[]{:S(2)}, u32[]{:S(2)}) collective-permute-start(bf16[15,512]{1,0:T(8,128)(2,1)S(1)} %get-tuple-element.8), channel_id=1, source_target_pairs={{0,8},{8,16},{16,24},{24,32},{32,40},{40,48},{48,56},{56,64},{64,7... | collective-permute-start | bytes 46088 | tf_op jit(solution)/shard_map/ppermute | solution.py:30
  112.6 111.3 %collective-permute-start.1 = (bf16[15,512]{1,0:T(8,128)(2,1)S(1)}, bf16[15,512]{1,0:T(8,128)(2,1)S(1)}, u32[]{:S(2)}, u32[]{:S(2)}) collective-permute-start(bf16[15,512]{1,0:T(8,128)(2,1)S(1)} %get-tuple-element.9), channel_id=1, source_target_pairs={{8,0},{16,8},{24,16},{32,24},{40,32},{48,40},{56,48},{64,56},{72,6... | collective-permute-start | bytes 46088 | tf_op jit(solution)/shard_map/ppermute | solution.py:33
Sparse Core Ops, SparseCore 0:
  11.6 94.8 all-gather.3
  109.6 84.0 all-gather.5
  196.7 79.1 all-gather.7
where the time goes:
time: 296 us
  waiting for transfers between devices  211 us (71%)
  matrix products  33.1 us (11%)
  other arithmetic  23.5 us (8%)
  between operations  14 us (5%)
  blocking collectives  8.59 us (3%)
  starting transfers between devices  3.33 us (1%)
    all_gather x1, waiting for transfers between devices, in_one_piece(): result = lax.all_gather(both, axis, axis=dim, tiled=True)  84.6 us
    all_gather x1, waiting for transfers between devices, per_device(): block_keys = lax.all_gather(own_keys, ('sp', 'tp'), axis=0, tiled=True)  76.4 us
    all_gather x1, waiting for transfers between devices, per_device(): lax.all_gather(out_weight, 'sp', axis=1, tiled=True)  49.8 us
    dot_general x1, matrix products, per_device(): jnp.einsum('hqc,kc->hqk', queries, block_keys, preferred_element_type=jnp...  10.9 us
    dot_general x1, matrix products, per_device(): jnp.einsum('htr,rhv->thv', attended, value_up.reshape(KVR, head_count, VD...  9.88 us
    reduce_sum x1, other arithmetic, per_device(): new_sum = jnp.sum(weights, axis=2)  8.7 us
    all_to_all x1, blocking collectives, sent_and_summed(): lax.all_to_all(tiles, axis, split_axis=0, concat_axis=0, tiled=True)  8.59 us
  transfers between devices with their start and end apart: 5, of which 3 were waited for; matrix products, arithmetic and copies ran while one was open for 18% of the time, Pallas kernels for 0%

commit v1 on v0

--- a/solution.py
+++ b/solution.py
@@ -167,7 +167,7 @@
     out_weight = jnp.concatenate([head_proj, channel_proj], axis=0)
     partial_terms = jnp.dot(
         mixed_in,
-        lax.all_gather(out_weight, "sp", axis=1, tiled=True),
+        jnp.concatenate(lax.all_gather(out_weight, "sp"), axis=1),
         preferred_element_type=jnp.float32,
     )
     mixed_out = sent_and_summed(partial_terms.astype(jnp.bfloat16), "tp", 1).astype(jnp.bfloat16)

time: 296 us -> 328 us (1.11)
  waiting for transfers between devices: 211 us -> 238 us
  local copies, waits for them, and re-layouts: 2.22 us -> 11.1 us
  blocking collectives: 8.59 us -> 4.07 us
    all_gather x1, waiting for transfers between devices: 49.8 us -> 77.3 us  [per_device(): lax.all_gather(out_weight, 'sp')]
    all_to_all x1, blocking collectives: 8.59 us -> 4.07 us  [sent_and_summed(): lax.all_to_all(tiles, axis, split_axis=0, concat_axis=0, tiled=True)]
    unnamed x8 -> x9, local copies, waits for them, and re-layouts: 0.28 us -> 4.79 us
    reshape x0 -> x1, local copies, waits for them, and re-layouts: none -> 4.34 us  [per_device(): jnp.concatenate(lax.all_gather(out_weight, 'sp'), axis=1)]
where the time goes in v1:
time: 328 us; the launch traced here: 327 us
  waiting for transfers between devices  238 us (73%)
  matrix products  33 us (10%)
  other arithmetic  23.4 us (7%)
  between operations  14.1 us (4%)
  local copies, waits for them, and re-layouts  11.1 us (3%)
  blocking collectives  4.07 us (1%)
  starting transfers between devices  3.33 us (1%)
    all_gather x1, waiting for transfers between devices, in_one_piece(): result = lax.all_gather(both, axis, axis=dim, tiled=True)  84.8 us
    all_gather x1, waiting for transfers between devices, per_device(): lax.all_gather(out_weight, 'sp')  77.3 us
    all_gather x1, waiting for transfers between devices, per_device(): block_keys = lax.all_gather(own_keys, ('sp', 'tp'), axis=0, tiled=True)  76.4 us
    dot_general x1, matrix products, per_device(): jnp.einsum('hqc,kc->hqk', queries, block_keys, preferred_element_type=jnp...  10.9 us
    dot_general x1, matrix products, per_device(): jnp.einsum('htr,rhv->thv', attended, value_up.reshape(KVR, head_count, VD...  9.83 us
    reduce_sum x1, other arithmetic, per_device(): new_sum = jnp.sum(weights, axis=2)  8.62 us
  transfers between devices with their start and end apart: 5, of which 3 were waited for; matrix products, arithmetic and copies ran while one was open for 18% of the time, Pallas kernels for 0%

profile of v1, /device:TPU:1, one launch (start us, length us, event | category | flops | bytes accessed | tf_op | source)
XLA Modules:
  0.0 327.4 jit_solution(17876910555709744722)
XLA Ops:
  7.2 1.5 pad_maximum_fusion.3
  8.8 1.4 pad_maximum_fusion.2
  11.8 1.2 fusion.32
  13.0 1.2 fusion.34
  14.8 1.2 fusion.53
  18.7 1.1 copy.72
  19.8 1.0 slice_convert_fusion.31
  20.8 1.0 slice_convert_fusion.32
  21.8 77.3 %all-gather.9.cloned.1.call-done = bf16[65536,32]{0,1:T(8,128)(2,1)} async-done(((bf16[1024,32]{0,1:T(8,128)(2,1)}), bf16[65536,32]{0,1:T(8,128)(2,1)}) %all-gather.9.cloned.1.call-update) | async-done | bytes 4194320 | tf_op jit(solution)/shard_map/all_gather | solution.py:170
  99.1 4.5 %copy.79 = bf16[4,8,64,1024]{3,2,1,0:T(8,128)(2,1)S(1)} copy(bf16[4,8,64,1024]{3,1,2,0:T(8,128)(2,1)} %bitcast.97) | data formatting | bytes 8388608
  103.6 4.3 %copy.66 = bf16[1024,64,32]{0,2,1:T(8,128)(2,1)} copy(bf16[1024,64,32]{0,1,2:T(8,128)(2,1)S(1)} %bitcast.96) | data formatting | bytes 8388608 | tf_op jit(solution)/shard_map/reshape | solution.py:170
  107.9 84.8 %all-gather.5.cloned.1.call-done = bf16[2048,1536]{1,0:T(8,128)(2,1)} async-done(((bf16[32,1536]{1,0:T(8,128)(2,1)}), bf16[2048,1536]{1,0:T(8,128)(2,1)}) %all-gather.5.cloned.1.call-update) | async-done | bytes 6291472 | tf_op jit(solution)/shard_map/all_gather | solution.py:21
  192.7 2.1 fusion.26
  194.8 2.1 fusion.29
  196.9 1.9 collective-permute-start
  198.8 1.3 collective-permute-start.1
  200.1 2.1 multiply_reduce_fusion.2
  203.5 76.4 %all-gather.7.cloned.1.call-done = bf16[8192,320]{1,0:T(8,128)(2,1)} async-done(((bf16[64,320]{1,0:T(8,128)(2,1)}), bf16[8192,320]{1,0:T(8,128)(2,1)}) %all-gather.7.cloned.1.call-update) | async-done | bytes 5242896 | tf_op jit(solution)/shard_map/all_gather | solution.py:130
  279.9 10.9 %multiply_reduce_fusion = (f32[4,128]{1,0:T(4,128)S(1)}, f32[4,128,8192]{2,1,0:T(8,128)}) fusion(bf16[8192,320]{1,0:T(8,128)(2,1)} %all-gather.7.cloned.1.call-done, bf16[4,128,64]{2,1,0:T(8,128)(2,1)S(1)} %maximum_bitcast_fusion, bf16[4,128,256]{2,1,0:T(8,128)(2,1)S(1)} %convolution_convert_fusion.1), kind=kOutput, calls=%fused_computation.1 | convolution fusion | flops 2693398016 | bytes 22349824 | tf_op jit(solution)/shard_map/hqc,kc->hqk/dot_general | solution.py:133
  290.8 8.6 %fusion = f32[4,128]{1,0:T(4,128)S(1)} fusion(f32[4,128,8192]{2,1,0:T(8,128)} %get-tuple-element.54, f32[4,128]{1,0:T(4,128)S(1)} %broadcast_maximum_fusion), kind=kLoop, calls=%fused_computation.2 | loop fusion | flops 12582400 | bytes 16781312 | tf_op jit(solution)/shard_map/reduce_sum | solution.py:138
  299.4 9.8 %convolution_convert_fusion.2 = bf16[4,128,128]{1,2,0:T(8,128)(2,1)S(1)} fusion(bf16[256,4,128]{0,2,1:T(8,128)(2,1)S(1)} %bitcast.104, bf16[8192,320]{1,0:T(8,128)(2,1)} %all-gather.7.cloned.1.call-done, f32[4,128,8192]{2,1,0:T(8,128)} %get-tuple-element.54, f32[4,128]{1,0:T(4,128)S(1)} %broadcast_maximum_fusion, f32[4,128]{1,0:T(4,128)S(1)} %fusion), kind=kOutput, calls=%fused_computation.26 | convolution fusion | flops 2193948672 | bytes 21368832 | tf_op jit(solution)/shard_map/htr,rhv->thv/dot_general | solution.py:159
  310.0 1.0 multiply_add_fusion
  312.2 3.7 %convolution_convert_fusion = bf16[128,2048]{1,0:T(8,128)(2,1)S(1)} fusion(bf16[1024,2048]{0,1:T(8,128)(2,1)} %bitcast.95, bf16[128,512]{1,0:T(8,128)(2,1)S(1)} %multiply_convert_fusion, bf16[128,512]{1,0:T(8,128)(2,1)S(1)} %copy.65), kind=kOutput, calls=%fused_computation.10 | convolution fusion | flops 537657344 | bytes 4980736 | tf_op jit(solution)/shard_map/dot_general | solution.py:168
  315.9 4.1 %all_to_all.5 = bf16[2,128,1024]{2,1,0:T(8,128)(2,1)S(1)} all-to-all(bf16[2,128,1024]{2,1,0:T(8,128)(2,1)S(1)} %bitcast.99), channel_id=1, replica_groups=mesh['sp'=64,'fs'=4,'tp'=2] {'tp'}, dimensions={0} | all-to-all | bytes 1048576 | tf_op jit(solution)/shard_map/all_to_all | solution.py:45
  (56 shorter events, 8.8 us)
Async XLA Ops:
  7.2 7.1 %copy-start = (bf16[2048,256]{1,0:T(8,128)(2,1)S(1)}, bf16[2048,256]{1,0:T(8,128)(2,1)}, u32[]{:S(2)}) copy-start(bf16[2048,256]{1,0:T(8,128)(2,1)} %param.20) | copy-start | bytes 3145732
  7.2 91.9 %all-gather.9.cloned.1.call-start = ((), (), s32[]{:S(2)}) async-start(), calls=%async_computation.3 | async-start | bytes 4259840 | tf_op jit(solution)/shard_map/all_gather | solution.py:170
  8.7 184.0 %all-gather.5.cloned.1.call-start = ((), (), s32[]{:S(2)}) async-start(), calls=%async_computation.1 | async-start | bytes 6389760 | tf_op jit(solution)/shard_map/all_gather | solution.py:21
  10.2 269.7 %all-gather.7.cloned.1.call-start = ((), (), s32[]{:S(2)}) async-start(), calls=%async_computation.2 | async-start | bytes 6340608 | tf_op jit(solution)/shard_map/all_gather | solution.py:130
  107.9 94.3 %copy-start.1 = (bf16[512,768]{1,0:T(8,128)(2,1)S(1)}, bf16[512,768]{1,0:T(8,128)(2,1)}, u32[]{:S(2)}) copy-start(bf16[512,768]{1,0:T(8,128)(2,1)} %param.23) | copy-start | bytes 2359300
  194.8 8.5 %copy-start.2 = (bf16[256,512]{1,0:T(8,128)(2,1)S(1)}, bf16[256,512]{1,0:T(8,128)(2,1)}, u32[]{:S(2)}) copy-start(bf16[256,512]{1,0:T(8,128)(2,1)} %param.24) | copy-start | bytes 786436
  196.9 113.0 %collective-permute-start = (bf16[15,512]{1,0:T(8,128)(2,1)S(1)}, bf16[15,512]{1,0:T(8,128)(2,1)S(1)}, u32[]{:S(2)}, u32[]{:S(2)}) collective-permute-start(bf16[15,512]{1,0:T(8,128)(2,1)S(1)} %get-tuple-element.8), channel_id=1, source_target_pairs={{0,8},{8,16},{16,24},{24,32},{32,40},{40,48},{48,56},{56,64},{64,7... | collective-permute-start | bytes 46088 | tf_op jit(solution)/shard_map/ppermute | solution.py:30
  198.8 111.1 %collective-permute-start.1 = (bf16[15,512]{1,0:T(8,128)(2,1)S(1)}, bf16[15,512]{1,0:T(8,128)(2,1)S(1)}, u32[]{:S(2)}, u32[]{:S(2)}) collective-permute-start(bf16[15,512]{1,0:T(8,128)(2,1)S(1)} %get-tuple-element.9), channel_id=1, source_target_pairs={{8,0},{16,8},{24,16},{32,24},{40,32},{48,40},{56,48},{64,56},{72,6... | collective-permute-start | bytes 46088 | tf_op jit(solution)/shard_map/ppermute | solution.py:33
Sparse Core Ops, SparseCore 0:
  11.0 88.0 all-gather.8
  102.7 89.9 all-gather.4
  195.8 84.0 all-gather.6
